TPU v7x, 256 devices: a 8x8x2 block of a 8x8x16 slice. The times are simulated.
256 devices in a mesh: grp: 2 (over z), ep: 64 (over y, x), tp: 2 (over core).
Axes of the slice: x: 8, y: 8, z: 2, core: 2. Of those that a mesh axis runs over, the one named last changes fastest.
The devices are a block of a 8x8x16 slice.
Arguments:
- tokens: bfloat16 [32768, 2048], P(('grp', 'ep', 'tp')), parts along dimension 0, may hold values from -6 to 6
- norm_gain: float32 [2048], replicated, may hold values from 0.1 to 1.9
- expert_ids: int32 [32768, 2], P(('grp', 'ep', 'tp')), parts along dimension 0, may hold values from 0 to 63, as said below
- gate_weights: float32 [32768, 2], P(('grp', 'ep', 'tp')), parts along dimension 0, may hold values from 0.1 to 1
- w_gate: bfloat16 [64, 2048, 512], P('ep', None, 'tp'), may hold values from -0.125 to 0.125
- w_up: bfloat16 [64, 2048, 512], P('ep', None, 'tp'), may hold values from -0.125 to 0.125
- w_down: bfloat16 [64, 512, 2048], P('ep', 'tp'), may hold values from -0.25 to 0.25
Outputs:
- mixed: bfloat16 [32768, 2048], P(('grp', 'ep', 'tp')), parts along dimension 0
There are 2 independent parts, one for each index of `grp`. A program takes and returns all parts, laid end to end along the dimension named above; an argument that names none is the same for every part. Nothing has to cross between parts.
Inputs may be any that keep to these rules, and one draw needn't show every extreme that they name: `expert_ids`: the 2 experts of a token are different and lie in one group of 16 consecutive experts. Among the rows of one device (aligned blocks of 128 rows) no expert is named more than 8 times, and in every such block some expert is named exactly 8 times.
All inputs are finite; a program needn't handle non-finite values.
Results may differ from a plain program's by a relative error of at most 0.0078.
Values may be sent and summed in bfloat16 or wider, within the bound.
A program may use at most 64 MiB of HBM per device.

v0:
```python
import jax
import jax.numpy as jnp
from jax import lax
from jax.sharding import PartitionSpec as P

N_GROUPS = 4


def normalize(tokens, norm_gain):
    values = tokens.astype(jnp.float32)
    scaled = values * lax.rsqrt(jnp.mean(values * values, axis=-1, keepdims=True) + 1e-06)
    return (scaled * norm_gain).astype(jnp.bfloat16)


def expert_whole(bucket_rows, full_gate, full_up, full_down, blocks):
    gate_act = jnp.einsum(
        "secd,edf->secf", bucket_rows, full_gate, preferred_element_type=jnp.float32
    )
    up_act = jnp.einsum("secd,edf->secf", bucket_rows, full_up, preferred_element_type=jnp.float32)
    hidden = (jax.nn.silu(gate_act) * up_act).astype(jnp.bfloat16)
    width = hidden.shape[-1] // blocks
    total = jnp.zeros(bucket_rows.shape, jnp.float32)
    for index in range(blocks):
        partial_value = jnp.einsum(
            "secf,efd->secd",
            hidden[..., index * width : (index + 1) * width],
            full_down[:, index * width : (index + 1) * width, :],
            preferred_element_type=jnp.float32,
        )
        rounded = lax.optimization_barrier(partial_value.astype(jnp.bfloat16))
        total = total + rounded.astype(jnp.float32)
    return total.astype(jnp.bfloat16)


def shards(tokens, norm_gain, expert_ids, gate_weights, w_gate, w_up, w_down):
    normed = normalize(tokens, norm_gain)
    n_tok, model_width = normed.shape
    top_count = expert_ids.shape[1]
    local_experts = w_gate.shape[0]
    n_ep = lax.axis_size("ep")
    n_tp = lax.axis_size("tp")
    n_exp = local_experts * n_ep
    capacity = top_count * (n_tok // 2) // (n_exp // N_GROUPS)
    total = n_tok * top_count
    n_slots = n_exp * capacity
    flat_e = expert_ids.reshape(-1)
    onehot = (flat_e[:, None] == jnp.arange(n_exp, dtype=jnp.int32)[None, :]).astype(jnp.bfloat16)
    positions = jnp.arange(total, dtype=jnp.int32)
    earlier = (positions[:, None] > positions[None, :]).astype(jnp.bfloat16)
    before = jnp.dot(earlier, onehot, preferred_element_type=jnp.float32)
    slot_index = jnp.sum(before * onehot.astype(jnp.float32), axis=1).astype(jnp.int32)
    dest_index = flat_e * capacity + slot_index
    slot_ids = jnp.arange(n_slots, dtype=jnp.int32)
    dispatch = (dest_index[None, :] == slot_ids[:, None]).astype(jnp.bfloat16)
    dispatch_tok = jnp.sum(dispatch.reshape(n_slots, n_tok, top_count), axis=2)
    buckets = jnp.dot(dispatch_tok, normed, preferred_element_type=jnp.float32).astype(jnp.bfloat16)
    buckets = buckets.reshape(n_exp, capacity, model_width)
    full_gate, full_up, full_down = (
        lax.all_gather(w_gate, "tp", axis=2, tiled=True),
        lax.all_gather(w_up, "tp", axis=2, tiled=True),
        lax.all_gather(w_down, "tp", axis=1, tiled=True),
    )
    received = lax.all_to_all(buckets, "ep", split_axis=0, concat_axis=0, tiled=True)
    grouped_rows = received.reshape(-1, local_experts, received.shape[1], model_width)
    computed = expert_whole(grouped_rows, full_gate, full_up, full_down, n_tp).reshape(
        received.shape
    )
    results = lax.all_to_all(computed, "ep", split_axis=0, concat_axis=0, tiled=True)
    results = results.reshape(n_slots, model_width)
    dest_pairs = dest_index.reshape(n_tok, top_count)
    mixed = jnp.zeros((n_tok, model_width), jnp.float32)
    for index in range(top_count):
        select = (dest_pairs[:, index][:, None] == slot_ids[None, :]).astype(jnp.bfloat16)
        picked = jnp.dot(select, results, preferred_element_type=jnp.float32)
        mixed = mixed + picked * gate_weights[:, index][:, None]
    return mixed.astype(jnp.bfloat16)


def solution(mesh):
    placed = (
        P(("grp", "ep", "tp"), None),
        P(),
        P(("grp", "ep", "tp"), None),
        P(("grp", "ep", "tp"), None),
        P("ep", None, "tp"),
        P("ep", None, "tp"),
        P("ep", "tp", None),
    )
    return jax.shard_map(
        shards, mesh=mesh, in_specs=placed, out_specs=P(("grp", "ep", "tp"), None), check_vma=False
    )
```

profile of v0, /device:TPU:646, one launch (start us, length us, event | category | flops | bytes accessed | tf_op | source)
XLA Modules:
  0.0 169.2 jit_solution(1217534860760275958)
XLA Ops:
  6.6 0.0 all-gather.4.cloned.1.call-start
  6.6 0.7 all-gather.4.cloned.1.call-update
  7.3 0.8 copy.19
  8.1 0.1 eq.59
  8.2 0.2 fusion.24
  8.5 0.1 convert_element_type.77
  8.6 0.1 copy.20
  8.7 0.7 multiply_add_fusion
  9.4 0.1 fusion.32
  9.4 1.2 fusion.25
  10.7 0.0 copy-done.1
  10.7 0.0 copy-done.2
  10.7 2.1 %fusion = bf16[64,8,2048]{2,1,0:T(8,128)(2,1)} fusion(bf16[512,128]{1,0:T(8,128)(2,1)S(1)} %fusion.32, bf16[128,2048]{1,0:T(8,128)(2,1)S(1)} %copy-done.1, f32[2048]{0:T(1024)S(1)} %copy-done.2, f32[128]{0:T(128)S(1)} %add_rsqrt_fusion), kind=kOutput, calls=%fused_computation.4 | convolution fusion | flops 270532608 | bytes 2761216 | tf_op jit(solution)/shard_map/dot_general | solution.py:56
  12.8 20.0 %all-to-all-start = ((bf16[64,8,2048]{2,1,0:T(8,128)(2,1)}), bf16[64,8,2048]{2,1,0:T(8,128)(2,1)S(1)}, u32[]{:S(2)}, u32[]{:S(2)}) async-start(bf16[64,8,2048]{2,1,0:T(8,128)(2,1)} %fusion), calls=%async_computation | async-start | bytes 4194304 | tf_op jit(solution)/shard_map/all_to_all | solution.py:63
  32.9 0.1 all-gather.6.cloned.1.call-start
  32.9 0.7 all-gather.6.cloned.1.call-update
  33.7 0.1 all-gather.8.cloned.1.call-start
  33.7 0.7 all-gather.8.cloned.1.call-update
  34.5 0.0 all-gather.4.cloned.1.call-done
  34.5 50.8 %all-to-all-done = bf16[64,8,2048]{2,1,0:T(8,128)(2,1)S(1)} async-done(((bf16[64,8,2048]{2,1,0:T(8,128)(2,1)}), bf16[64,8,2048]{2,1,0:T(8,128)(2,1)S(1)}, u32[]{:S(2)}, u32[]{:S(2)}) %all-to-all-start) | async-done | bytes 2097184 | tf_op jit(solution)/shard_map/all_to_all | solution.py:63
  85.3 3.9 %fusion.12 = f32[64,1,8,512]{3,2,0,1:T(8,128)} fusion(bf16[64,8,2048]{2,1,0:T(8,128)(2,1)S(1)} %all-to-all-done, bf16[1,2048,512]{2,1,0:T(8,128)(2,1)} %all-gather.4.cloned.1.call-done), kind=kOutput, calls=%fused_computation.18 | convolution fusion | flops 1073741824 | bytes 5242880 | tf_op jit(solution)/shard_map/secd,edf->secf/dot_general | solution.py:16
  89.2 3.2 %fusion.21 = bf16[64,1,8,512]{3,2,0,1:T(8,128)(2,1)S(1)} fusion(bf16[64,8,2048]{2,1,0:T(8,128)(2,1)S(1)} %all-to-all-done, bf16[1,2048,512]{2,1,0:T(8,128)(2,1)} %all-gather.6.cloned.1.call-done, f32[64,1,8,512]{3,2,0,1:T(8,128)} %fusion.12), kind=kOutput, calls=%fused_computation.23 | convolution fusion | flops 1075314688 | bytes 5767168 | tf_op jit(solution)/shard_map/secd,edf->secf/dot_general | solution.py:19
  92.4 0.0 all-gather.8.cloned.1.call-done
  92.4 0.0 copy-start
  92.4 2.1 %fusion.1 = bf16[64,1,8,2048]{3,2,0,1:T(8,128)(2,1)S(1)} fusion(bf16[1,512,2048]{2,1,0:T(8,128)(2,1)} %all-gather.8.cloned.1.call-done, bf16[64,1,8,512]{3,2,0,1:T(8,128)(2,1)S(1)} %fusion.21), kind=kOutput, calls=%fused_computation.5 | convolution fusion | flops 537919488 | bytes 3407872 | tf_op jit(solution)/shard_map/secf,efd->secd/dot_general | solution.py:24
  94.5 0.7 fusion.2
  95.3 2.2 %fusion.5 = bf16[64,8,2048]{2,1,0:T(8,128)(2,1)} fusion(bf16[64,1,8,2048]{3,2,0,1:T(8,128)(2,1)S(1)} %fusion.2, bf16[64,1,8,2048]{3,2,0,1:T(8,128)(2,1)S(1)} %fusion.1), kind=kLoop, calls=%fused_computation.11 | loop fusion | flops 4194304 | bytes 6291456 | tf_op jit(solution)/shard_map/reshape | solution.py:65
  97.4 9.7 %all-to-all-start.1 = ((bf16[64,8,2048]{2,1,0:T(8,128)(2,1)}), bf16[64,8,2048]{2,1,0:T(8,128)(2,1)S(1)}, u32[]{:S(2)}, u32[]{:S(2)}) async-start(bf16[64,8,2048]{2,1,0:T(8,128)(2,1)} %fusion.5), calls=%async_computation.1 | async-start | bytes 4194304 | tf_op jit(solution)/shard_map/all_to_all | solution.py:68
  107.1 0.0 copy-done.3
  107.1 53.7 %all-to-all-done.1 = bf16[64,8,2048]{2,1,0:T(8,128)(2,1)S(1)} async-done(((bf16[64,8,2048]{2,1,0:T(8,128)(2,1)}), bf16[64,8,2048]{2,1,0:T(8,128)(2,1)S(1)}, u32[]{:S(2)}, u32[]{:S(2)}) %all-to-all-start.1) | async-done | bytes 2097184 | tf_op jit(solution)/shard_map/all_to_all | solution.py:68
  160.8 0.5 convolution_multiply_fusion.1
  161.3 1.3 fusion.4
  (9 shorter events, 0.0 us)
Async XLA Ops:
  6.5 4.1 %copy-start.1 = (bf16[128,2048]{1,0:T(8,128)(2,1)S(1)}, bf16[128,2048]{1,0:T(8,128)(2,1)}, u32[]{:S(2)}) copy-start(bf16[128,2048]{1,0:T(8,128)(2,1)} %param.7) | copy-start | bytes 1572868
  6.5 4.1 %copy-start.2 = (f32[2048]{0:T(1024)S(1)}, f32[2048]{0:T(1024)}, u32[]{:S(2)}) copy-start(f32[2048]{0:T(1024)} %param.8) | copy-start | bytes 24580
  6.6 27.9 %all-gather.4.cloned.1.call-start = ((), (), s32[]{:S(2)}) async-start(), calls=%async_computation.2 | async-start | bytes 3145728 | tf_op jit(solution)/shard_map/all_gather | solution.py:59
  12.8 72.5 %all-to-all-start = ((bf16[64,8,2048]{2,1,0:T(8,128)(2,1)}), bf16[64,8,2048]{2,1,0:T(8,128)(2,1)S(1)}, u32[]{:S(2)}, u32[]{:S(2)}) async-start(bf16[64,8,2048]{2,1,0:T(8,128)(2,1)} %fusion), calls=%async_computation | async-start | bytes 4194304 | tf_op jit(solution)/shard_map/all_to_all | solution.py:63
  32.9 56.3 %all-gather.6.cloned.1.call-start = ((), (), s32[]{:S(2)}) async-start(), calls=%async_computation.3 | async-start | bytes 3145728 | tf_op jit(solution)/shard_map/all_gather | solution.py:60
  33.7 58.7 %all-gather.8.cloned.1.call-start = ((), (), s32[]{:S(2)}) async-start(), calls=%async_computation.4 | async-start | bytes 3145728 | tf_op jit(solution)/shard_map/all_gather | solution.py:61
  92.4 2.1 %copy-start = (bf16[1,512,2048]{2,1,0:T(8,128)(2,1)S(1)}, bf16[1,512,2048]{2,1,0:T(8,128)(2,1)}, u32[]{:S(2)}) copy-start(bf16[1,512,2048]{2,1,0:T(8,128)(2,1)} %all-gather.8.cloned.1.call-done) | copy-start | bytes 6291460
  97.4 9.7 %copy-start.3 = (f32[128,2]{0,1:T(2,128)S(1)}, f32[128,2]{0,1:T(2,128)}, u32[]{:S(2)}) copy-start(f32[128,2]{0,1:T(2,128)} %param.10) | copy-start | bytes 3076
  97.4 63.4 %all-to-all-start.1 = ((bf16[64,8,2048]{2,1,0:T(8,128)(2,1)}), bf16[64,8,2048]{2,1,0:T(8,128)(2,1)S(1)}, u32[]{:S(2)}, u32[]{:S(2)}) async-start(bf16[64,8,2048]{2,1,0:T(8,128)(2,1)} %fusion.5), calls=%async_computation.1 | async-start | bytes 4194304 | tf_op jit(solution)/shard_map/all_to_all | solution.py:68
Sparse Core Ops, SparseCore 0:
  9.2 24.5 all-gather.3
  35.6 18.2 all-gather.5
  55.7 18.7 all-gather.7
where the time goes:
time: 170 us; the launch traced here: 169 us
  waiting for transfers between devices  107 us (63%)
  starting transfers between devices  29.8 us (18%)
  matrix products  14 us (8%)
  between operations  13.3 us (8%)
  other arithmetic  4.17 us (2%)
    all_to_all x1, waiting for transfers between devices, shards(): lax.all_to_all(computed, 'ep', split_axis=0, concat_axis=0, tiled=True)  53.7 us
    all_to_all x1, waiting for transfers between devices, shards(): lax.all_to_all(buckets, 'ep', split_axis=0, concat_axis=0, tiled=True)  50.8 us
    all_to_all x1, starting transfers between devices, shards(): lax.all_to_all(buckets, 'ep', split_axis=0, concat_axis=0, tiled=True)  20 us
    all_to_all x1, starting transfers between devices, shards(): lax.all_to_all(computed, 'ep', split_axis=0, concat_axis=0, tiled=True)  9.68 us
    dot_general x1, matrix products, expert_whole(): jnp.einsum('secd,edf->secf', bucket_rows, full_gate, preferred_element_ty...  3.86 us
  transfers between devices with their start and end apart: 5, of which 2 were waited for; matrix products, arithmetic and copies ran while one was open for 7% of the time, Pallas kernels for 0%

commit v1 on v0

v1 whole, which is shorter than its diff:
```python
import functools
import math

import jax
import jax.numpy as jnp
from jax import lax
from jax.experimental import pallas as pl
from jax.experimental.pallas import tpu as pltpu
from jax.sharding import PartitionSpec as P

N_GROUPS = 4
BLOCKS = 4
MESH = pl.DeviceIdType.MESH
BF16 = jnp.bfloat16
F32 = jnp.float32


def kernel(
    n_ep,
    side,
    cap,
    tokens_ref,
    gain_ref,
    ids_ref,
    gates_ref,
    wg_hbm,
    wu_hbm,
    wd_hbm,
    out_ref,
    normed,
    pick0,
    pick1,
    buckets,
    recv,
    outs,
    results,
    wg,
    wu,
    wd,
    acc,
    local_sem,
    wsend_sem,
    wrecv_sem,
    dsend_sem,
    drecv_sem,
    csend_sem,
    crecv_sem,
):
    ep = lax.axis_index("ep")
    tp = lax.axis_index("tp")
    my, mx = ep // side, lax.rem(ep, side)
    per_block = n_ep // BLOCKS
    rows = per_block * cap
    n_tok = tokens_ref.shape[0]
    n_slots = n_ep * cap

    def offset(o):
        block, j = o // per_block, lax.rem(o, per_block)
        dx = j // 2
        dy = lax.rem(block + side - dx, BLOCKS) + BLOCKS * lax.rem(j, 2)
        return dy, dx

    def ahead(o):
        dy, dx = offset(o)
        return lax.rem(my + dy, side) * side + lax.rem(mx + dx, side)

    def behind(o):
        dy, dx = offset(o)
        return lax.rem(my + side - dy, side) * side + lax.rem(mx + side - dx, side)

    barrier = pltpu.get_barrier_semaphore()

    @pl.loop(1, n_ep)
    def _(i):
        pl.semaphore_signal(
            barrier, inc=1, device_id={"ep": lax.rem(ep + i, n_ep)}, device_id_type=MESH
        )

    pl.semaphore_signal(barrier, inc=1, device_id={"tp": 1 - tp}, device_id_type=MESH)

    local = [
        pltpu.make_async_copy(src.at[0], dst.at[tp], local_sem.at[i])
        for i, (src, dst) in enumerate(((wg_hbm, wg), (wu_hbm, wu), (wd_hbm, wd)))
    ]
    for copy in local:
        copy.start()

    values = tokens_ref[...].astype(F32)
    scale = lax.rsqrt(jnp.mean(values * values, axis=-1, keepdims=True) + 1e-06)
    normed[...] = (values * scale * gain_ref[...]).astype(BF16)

    ids = ids_ref[...]
    experts = [ids[:, k : k + 1] for k in range(ids.shape[1])]
    lanes = lax.broadcasted_iota(jnp.int32, (n_tok, n_ep), 1)
    hots = [(e == lanes).astype(F32) for e in experts]
    earlier = (
        lax.broadcasted_iota(jnp.int32, (n_tok, n_tok), 0)
        > lax.broadcasted_iota(jnp.int32, (n_tok, n_tok), 1)
    ).astype(BF16)
    before = jnp.dot(earlier, sum(hots).astype(BF16), preferred_element_type=F32)
    slots = lax.broadcasted_iota(jnp.int32, (n_tok, n_slots), 1)
    for e, hot, pick in zip(experts, hots, (pick0, pick1)):
        place = jnp.sum(before * hot, axis=1, keepdims=True).astype(jnp.int32)
        dy = (e // side - my + side) % side
        dx = (e % side - mx + side) % side
        order = (dx + dy) % BLOCKS * per_block + dx * 2 + dy // BLOCKS
        hot_slot = (order * cap + place == slots).astype(BF16)
        for b in range(BLOCKS):
            pick[b] = hot_slot[:, b * rows : (b + 1) * rows]

    def bucket(b):
        block = pl.ds(b * rows, rows)
        buckets[block, :] = lax.dot_general(
            pick0[b] + pick1[b], normed[...], (((0,), (0,)), ((), ())), preferred_element_type=F32
        ).astype(BF16)

    def part(o):
        return pl.ds(pl.multiple_of(o * cap, cap), cap)

    def dispatch(o):
        return pltpu.make_async_remote_copy(
            src_ref=buckets.at[part(o)],
            dst_ref=recv.at[part(o)],
            send_sem=dsend_sem.at[o],
            recv_sem=drecv_sem.at[o],
            device_id={"ep": ahead(o)},
            device_id_type=MESH,
        )

    def giveback(o):
        return pltpu.make_async_remote_copy(
            src_ref=outs.at[part(o)],
            dst_ref=results.at[part(o)],
            send_sem=csend_sem.at[o],
            recv_sem=crecv_sem.at[o],
            device_id={"ep": behind(o)},
            device_id_type=MESH,
        )

    def shuffled(b, j):
        return b * per_block + lax.rem(j * 5 + mx * 3 + my * 7, per_block)

    def send_block(make, b):
        @pl.loop(0, per_block)
        def _(j):
            o = shuffled(b, j)

            @pl.when(o != 0)
            def _():
                make(o).start()

    def await_block(make, b):
        @pl.loop(0, per_block)
        def _(j):
            o = b * per_block + j

            @pl.when(o != 0)
            def _():
                make(o).wait_recv()

    bucket(0)
    pl.semaphore_wait(barrier, n_ep)
    send_block(dispatch, 0)
    for copy in local:
        copy.wait()
    swaps = [
        pltpu.make_async_remote_copy(
            src_ref=ref.at[tp],
            dst_ref=ref.at[tp],
            send_sem=wsend_sem.at[i],
            recv_sem=wrecv_sem.at[i],
            device_id={"tp": 1 - tp},
            device_id_type=MESH,
        )
        for i, ref in enumerate((wg, wu, wd))
    ]
    for swap in swaps:
        swap.start()

    @pl.loop(1, BLOCKS)
    def _(b):
        bucket(b)
        send_block(dispatch, b)

    recv[:cap, :] = buckets[:cap, :]
    for swap in swaps:
        swap.wait()

    @pl.loop(0, BLOCKS)
    def _(b):
        await_block(dispatch, b)
        block = pl.ds(b * rows, rows)
        taken = recv[block, :]
        total = None
        for j in range(wg.shape[0]):
            gate_act = jnp.dot(taken, wg[j], preferred_element_type=F32)
            up_act = jnp.dot(taken, wu[j], preferred_element_type=F32)
            hidden = (gate_act / (1.0 + jnp.exp(-gate_act)) * up_act).astype(BF16)
            partial = jnp.dot(hidden, wd[j], preferred_element_type=F32).astype(BF16).astype(F32)
            total = partial if total is None else total + partial
        outs[block, :] = total.astype(BF16)
        send_block(giveback, b)

    results[:cap, :] = outs[:cap, :]
    gates = gates_ref[...]
    acc[...] = jnp.zeros_like(acc)

    @pl.loop(0, BLOCKS)
    def _(b):
        await_block(giveback, b)
        back = results[pl.ds(b * rows, rows), :]
        acc[...] += (
            jnp.dot(pick0[b], back, preferred_element_type=F32) * gates[:, 0:1]
            + jnp.dot(pick1[b], back, preferred_element_type=F32) * gates[:, 1:2]
        )

    out_ref[...] = acc[...].astype(BF16)

    @pl.loop(1, n_ep)
    def _(o):
        dispatch(o).wait_send()
        giveback(o).wait_send()


def shards(n_ep, n_tp, tokens, norm_gain, expert_ids, gate_weights, w_gate, w_up, w_down):
    n_tok, width = tokens.shape
    top_count = expert_ids.shape[1]
    n_exp = w_gate.shape[0] * n_ep
    side = math.isqrt(n_ep)
    cap = top_count * (n_tok // 2) // (n_exp // N_GROUPS)
    n_slots = n_exp * cap
    rows = n_slots // BLOCKS
    hidden = w_gate.shape[2]
    vmem = pl.BlockSpec(memory_space=pltpu.VMEM)
    anywhere = pl.BlockSpec(memory_space=pl.ANY)
    dma = pltpu.SemaphoreType.DMA
    return pl.pallas_call(
        functools.partial(kernel, n_ep, side, cap),
        out_shape=jax.ShapeDtypeStruct((n_tok, width), BF16),
        in_specs=[vmem] * 4 + [anywhere] * 3,
        out_specs=vmem,
        scratch_shapes=[
            pltpu.VMEM((n_tok, width), BF16),
            pltpu.VMEM((BLOCKS, n_tok, rows), BF16),
            pltpu.VMEM((BLOCKS, n_tok, rows), BF16),
            pltpu.VMEM((n_slots, width), BF16),
            pltpu.VMEM((n_slots, width), BF16),
            pltpu.VMEM((n_slots, width), BF16),
            pltpu.VMEM((n_slots, width), BF16),
            pltpu.VMEM((n_tp, width, hidden), BF16),
            pltpu.VMEM((n_tp, width, hidden), BF16),
            pltpu.VMEM((n_tp, hidden, width), BF16),
            pltpu.VMEM((n_tok, width), F32),
            dma((3,)),
            dma((3,)),
            dma((3,)),
            dma((n_ep,)),
            dma((n_ep,)),
            dma((n_ep,)),
            dma((n_ep,)),
        ],
        compiler_params=pltpu.CompilerParams(
            collective_id=0, has_side_effects=True, vmem_limit_bytes=60 * 1024 * 1024
        ),
    )(tokens, norm_gain.reshape(1, width), expert_ids, gate_weights, w_gate, w_up, w_down)


def solution(mesh):
    placed = (
        P(("grp", "ep", "tp"), None),
        P(),
        P(("grp", "ep", "tp"), None),
        P(("grp", "ep", "tp"), None),
        P("ep", None, "tp"),
        P("ep", None, "tp"),
        P("ep", "tp", None),
    )
    return jax.shard_map(
        functools.partial(shards, mesh.shape["ep"], mesh.shape["tp"]),
        mesh=mesh,
        in_specs=placed,
        out_specs=P(("grp", "ep", "tp"), None),
        check_vma=False,
    )
```

time: 170 us -> 137 us (0.81)
  the two profiles are of different devices: /device:TPU:646 before, /device:TPU:518 now
where the time goes in v1:
time: 137 us; the launch traced here: 135 us
  Pallas kernels  131 us (96%)
  local copies, waits for them, and re-layouts  4.03 us (3%)
    pallas_call x1, Pallas kernels, shards(): pl.pallas_call(functools.partial(kernel, n_ep, side, cap), out_shape=jax....  131 us
    unnamed x7, local copies, waits for them, and re-layouts  4.03 us

profile of v1, /device:TPU:518, one launch (start us, length us, event | category | flops | bytes accessed | tf_op | source)
XLA Modules:
  0.0 135.1 jit_solution(1510444247310561734)
XLA Ops:
  0.0 0.0 copy-start
  0.0 0.7 copy-done
  0.7 0.0 copy-start.1
  0.7 0.7 copy.8.ids_ref
  1.4 0.0 copy-done.1
  1.4 0.7 copy.9.gates_ref
  2.2 131.0 %shard_map.73 = bf16[128,2048]{1,0:T(8,128)(2,1)} custom-call(bf16[128,2048]{1,0:T(8,128)(2,1)} %tokens_ref.1, f32[1,2048]{1,0:T(1,128)} %bitcast.1, s32[128,2]{1,0:T(8,128)} %copy.8.ids_ref, f32[128,2]{1,0:T(8,128)} %copy.9.gates_ref, bf16[1,2048,256]{2,1,0:T(8,128)(2,1)} %wg_hbm.1, bf16[1,2048,256]{2,1,0:T(8,128)(2,1)} %wu_hbm.1, bf16[1,256,2048]{2,1,0:T(8,128)(2,1)} %wd_hbm.1), custom_call_target="tpu_custom_call" | custom-call | tf_op jit(solution)/shard_map/pallas_call | solution.py:237
  133.2 1.9 %copy.11 = bf16[128,2048]{1,0:T(8,128)(2,1)} copy(bf16[128,2048]{1,0:T(8,128)(2,1)} %shard_map.73) | data formatting | bytes 1048576
Async XLA Ops:
  0.0 0.7 copy-start
  0.7 0.7 copy-start.1

commit v2 on v1

v2 whole, which is shorter than its diff:
```python
import functools
import math

import jax
import jax.numpy as jnp
from jax import lax
from jax.experimental import pallas as pl
from jax.experimental.pallas import tpu as pltpu
from jax.sharding import PartitionSpec as P

N_GROUPS = 4
MESH = pl.DeviceIdType.MESH
BF16 = jnp.bfloat16
F32 = jnp.float32


def kernel(
    side,
    cap,
    cut,
    tokens_ref,
    gain_ref,
    ids_ref,
    gates_ref,
    wg_hbm,
    wu_hbm,
    wd_hbm,
    out_ref,
    pick,
    weigh_hi,
    weigh_lo,
    bkt_a,
    bkt_b,
    mid_a,
    mid_b,
    recv_a,
    recv_b,
    outs_a,
    outs_b,
    back_a,
    back_b,
    res_a,
    res_b,
    wg,
    wu,
    wd,
    acc,
    local_sem,
    swap_sem,
    line_sem,
    turn_a_sem,
    turn_b_sem,
):
    n_ep = side * side
    half = side // 2
    pairs = half
    ep = lax.axis_index("ep")
    tp = lax.axis_index("tp")
    my, mx = ep // side, lax.rem(ep, side)
    n_tok = tokens_ref.shape[0]
    rows = 2 * side * cap

    def shift(p):
        k = p // 2
        return jnp.where(p % 2 == 0, k, jnp.where(k == 0, half, side - k))

    def in_row(p, sign):
        return my * side + lax.rem(mx + side + sign * shift(p), side)

    def in_column(q, sign):
        return lax.rem(my + side + sign * shift(q), side) * side + mx

    def remote(src, dst, sems, at, target):
        return pltpu.make_async_remote_copy(
            src_ref=src,
            dst_ref=dst,
            send_sem=sems.at[(0, *at)],
            recv_sem=sems.at[(1, *at)],
            device_id={"ep": target},
            device_id_type=MESH,
        )

    def out1_a(p):
        return remote(bkt_a.at[p], mid_a.at[p], line_sem, (0, p), in_row(p, 1))

    def out1_b(q):
        return remote(bkt_b.at[q], mid_b.at[q], line_sem, (1, q), in_column(q, 1))

    def out2_a(c, q):
        two = pl.ds(2 * c, 2)
        return remote(mid_a.at[two, q], recv_a.at[two, q], turn_a_sem, (0, c, q), in_column(q, 1))

    def out2_b(h, p):
        some = pl.ds(h * half, half)
        return remote(mid_b.at[some, p], recv_b.at[p, some], turn_b_sem, (h, p), in_row(p, 1))

    def in1_a(c, q):
        two = pl.ds(2 * c, 2)
        return remote(outs_a.at[two, q], back_a.at[two, q], turn_a_sem, (1, c, q), in_column(q, -1))

    def in1_b(p):
        return remote(outs_b.at[p], back_b.at[p], line_sem, (2, p), in_row(p, -1))

    def in2_a(p):
        return remote(back_a.at[p], res_a.at[p], line_sem, (3, p), in_row(p, -1))

    def in2_b(c, q):
        two = pl.ds(2 * c, 2)
        return remote(back_b.at[two, q], res_b.at[two, q], turn_a_sem, (2, c, q), in_column(q, -1))

    barrier = pltpu.get_barrier_semaphore()

    @pl.loop(1, side)
    def _(p):
        pl.semaphore_signal(barrier, inc=1, device_id={"ep": in_row(p, 1)}, device_id_type=MESH)
        pl.semaphore_signal(barrier, inc=1, device_id={"ep": in_column(p, 1)}, device_id_type=MESH)

    pl.semaphore_signal(barrier, inc=1, device_id={"tp": 1 - tp}, device_id_type=MESH)

    local = [
        pltpu.make_async_copy(src.at[0], dst.at[tp], local_sem.at[i])
        for i, (src, dst) in enumerate(((wg_hbm, wg), (wu_hbm, wu), (wd_hbm, wd)))
    ]
    for copy in local:
        copy.start()

    ids = ids_ref[...]
    gates = gates_ref[...]
    below = lax.broadcasted_iota(jnp.int32, (n_ep, n_tok), 0)
    hots = [(ids[k : k + 1] == below).astype(F32) for k in range(ids.shape[0])]
    earlier = (
        lax.broadcasted_iota(jnp.int32, (n_tok, n_tok), 0)
        < lax.broadcasted_iota(jnp.int32, (n_tok, n_tok), 1)
    ).astype(BF16)
    before = jnp.dot(sum(hots).astype(BF16), earlier, preferred_element_type=F32)

    def place(d):
        return jnp.where(d == 0, 0, jnp.where(d == half, 1, jnp.where(d < half, 2 * d, 2 * (side - d) + 1)))

    slots = []
    for k, hot in enumerate(hots):
        e = ids[k : k + 1]
        nth = jnp.sum(before * hot, axis=0, keepdims=True).astype(jnp.int32)
        q = place((e // side - my + side) % side)
        p = place((e % side - mx + side) % side)
        slots.append((p * side + q) * cap + nth)
    gates_hi = gates.astype(BF16).astype(F32)
    gates_lo = gates - gates_hi
    for c in range(pairs):
        row = lax.broadcasted_iota(jnp.int32, (rows, n_tok), 0) + c * rows
        picks = [slot == row for slot in slots]
        pick[c] = sum(x.astype(F32) for x in picks).astype(BF16)
        for weigh, g in ((weigh_hi, gates_hi), (weigh_lo, gates_lo)):
            weigh[c] = sum(jnp.where(x, g[k : k + 1], 0.0) for k, x in enumerate(picks)).astype(BF16)

    values = tokens_ref[...].astype(F32)
    scale = lax.rsqrt(jnp.mean(values * values, axis=-1, keepdims=True) + 1e-06)
    normed = (values * scale * gain_ref[...]).astype(BF16)
    for c in range(pairs):
        bucket = jnp.dot(pick[c], normed, preferred_element_type=F32).astype(BF16)
        bkt_a[pl.ds(2 * c, 2)] = bucket[:, :cut].reshape(2, side, cap, cut)
        for i in range(2):
            bkt_b[:, 2 * c + i] = bucket[i * (rows // 2) : (i + 1) * (rows // 2), cut:].reshape(side, cap, -1)

    pl.semaphore_wait(barrier, 2 * side - 1)

    @pl.loop(1, side)
    def _(p):
        out1_a(p).start()
        out1_b(p).start()

    for copy in local:
        copy.wait()
    swaps = [
        pltpu.make_async_remote_copy(
            src_ref=ref.at[tp],
            dst_ref=ref.at[tp],
            send_sem=swap_sem.at[0, i],
            recv_sem=swap_sem.at[1, i],
            device_id={"tp": 1 - tp},
            device_id_type=MESH,
        )
        for i, ref in enumerate((wg, wu, wd))
    ]
    for swap in swaps:
        swap.start()

    mid_a[0] = bkt_a[0]
    mid_b[0] = bkt_b[0]

    def turn_b(h):
        @pl.loop(max(1, h * half), (h + 1) * half)
        def _(q):
            out1_b(q).wait_recv()

        @pl.loop(1, side)
        def _(p):
            out2_b(h, p).start()

    def turn_a(c):
        if c:
            out1_a(2 * c).wait_recv()
        out1_a(2 * c + 1).wait_recv()

        @pl.loop(1, side)
        def _(q):
            out2_a(c, q).start()

    for c in range(pairs):
        turn_a(c)
        if c % 2:
            turn_b(c // 2)

    recv_a[:, 0] = mid_a[:, 0]
    recv_b[0] = mid_b[:, 0]
    for swap in swaps:
        swap.wait()

    @pl.loop(0, pairs)
    def _(c):
        @pl.loop(1, side)
        def _(q):
            out2_a(c, q).wait_recv()

        @pl.when(c > 0)
        def _():
            for h in range(2):
                out2_b(h, 2 * c).wait_recv()

        for h in range(2):
            out2_b(h, 2 * c + 1).wait_recv()

        two = pl.ds(2 * c, 2)
        taken_a = recv_a[two].reshape(rows, -1)
        taken_b = recv_b[two].reshape(rows, -1)
        total = None
        for j in range(wg.shape[0]):
            gate_act, up_act = (
                jnp.dot(taken_a, w[j, :cut], preferred_element_type=F32)
                + jnp.dot(taken_b, w[j, cut:], preferred_element_type=F32)
                for w in (wg, wu)
            )
            hidden = (gate_act / (1.0 + jnp.exp(-gate_act)) * up_act).astype(BF16)
            partial = jnp.dot(hidden, wd[j], preferred_element_type=F32).astype(BF16).astype(F32)
            total = partial if total is None else total + partial
        total = total.astype(BF16)
        outs_a[two] = total[:, :cut].reshape(2, side, cap, cut)
        outs_b[two] = total[:, cut:].reshape(2, side, cap, -1)

        @pl.loop(1, side)
        def _(q):
            in1_a(c, q).start()

        @pl.when(c > 0)
        def _():
            in1_b(2 * c).start()

        in1_b(2 * c + 1).start()

    back_a[:, 0] = outs_a[:, 0]
    back_b[0] = outs_b[0]

    for c in range(pairs):
        if c:
            in1_b(2 * c).wait_recv()
        in1_b(2 * c + 1).wait_recv()

        @pl.loop(1, side)
        def _(q):
            in2_b(c, q).start()
            in1_a(c, q).wait_recv()

        if c:
            in2_a(2 * c).start()
        in2_a(2 * c + 1).start()

    res_a[0] = back_a[0]
    res_b[:, 0] = back_b[:, 0]

    for c in range(pairs):
        if c:
            in2_a(2 * c).wait_recv()
        in2_a(2 * c + 1).wait_recv()

        @pl.loop(1, side)
        def _(q):
            in2_b(c, q).wait_recv()

        two = pl.ds(2 * c, 2)
        for res, span in ((res_a, pl.ds(0, cut)), (res_b, pl.ds(cut, tokens_ref.shape[1] - cut))):
            value = res[two].reshape(rows, -1)
            got = sum(
                lax.dot_general(w[c], value, (((0,), (0,)), ((), ())), preferred_element_type=F32)
                for w in (weigh_hi, weigh_lo)
            )
            if c:
                got = got + acc[:, span]
            if c < pairs - 1:
                acc[:, span] = got
            else:
                out_ref[:, span] = got.astype(out_ref.dtype)

    @pl.loop(1, side)
    def _(p):
        for make in (out1_a, out1_b, in1_b, in2_a):
            make(p).wait_send()
        for h in range(2):
            out2_b(h, p).wait_send()
        for c in range(pairs):
            out2_a(c, p).wait_send()
            in1_a(c, p).wait_send()
            in2_b(c, p).wait_send()


def shards(n_ep, n_tp, tokens, norm_gain, expert_ids, gate_weights, w_gate, w_up, w_down):
    n_tok, width = tokens.shape
    top_count = expert_ids.shape[1]
    n_exp = w_gate.shape[0] * n_ep
    side = math.isqrt(n_ep)
    cap = top_count * (n_tok // 2) // (n_exp // N_GROUPS)
    cut = width // 2
    rows = 2 * side * cap
    hidden = w_gate.shape[2]
    vmem = pl.BlockSpec(memory_space=pltpu.VMEM)
    anywhere = pl.BlockSpec(memory_space=pl.ANY)
    dma = pltpu.SemaphoreType.DMA
    part_a = pltpu.VMEM((side, side, cap, cut), BF16)
    part_b = pltpu.VMEM((side, side, cap, width - cut), BF16)
    mixed = pl.pallas_call(
        functools.partial(kernel, side, cap, cut),
        out_shape=jax.ShapeDtypeStruct((n_tok, width), BF16),
        in_specs=[vmem] * 4 + [anywhere] * 3,
        out_specs=vmem,
        scratch_shapes=[
            *([pltpu.VMEM((side // 2, rows, n_tok), BF16)] * 3),
            *([part_a, part_b] * 6),
            pltpu.VMEM((n_tp, width, hidden), BF16),
            pltpu.VMEM((n_tp, width, hidden), BF16),
            pltpu.VMEM((n_tp, hidden, width), BF16),
            pltpu.VMEM((n_tok, width), F32),
            dma((3,)),
            dma((2, 3)),
            dma((2, 4, side)),
            dma((2, 3, side // 2, side)),
            dma((2, 2, side)),
        ],
        compiler_params=pltpu.CompilerParams(
            collective_id=0, has_side_effects=True, vmem_limit_bytes=60 * 1024 * 1024
        ),
    )(tokens, norm_gain.reshape(1, width), expert_ids.T, gate_weights.T, w_gate, w_up, w_down)
    return mixed


def solution(mesh):
    placed = (
        P(("grp", "ep", "tp"), None),
        P(),
        P(("grp", "ep", "tp"), None),
        P(("grp", "ep", "tp"), None),
        P("ep", None, "tp"),
        P("ep", None, "tp"),
        P("ep", "tp", None),
    )
    return jax.shard_map(
        functools.partial(shards, mesh.shape["ep"], mesh.shape["tp"]),
        mesh=mesh,
        in_specs=placed,
        out_specs=P(("grp", "ep", "tp"), None),
        check_vma=False,
    )
```

time: 137 us -> 116 us (0.85); the launches traced: 135 us -> 115 us
  Pallas kernels: 131 us -> 114 us
  local copies, waits for them, and re-layouts: 4.03 us -> 1.88 us
    pallas_call x1, Pallas kernels: 131 us -> 114 us  [shards(): pl.pallas_call(functools.partial(kernel, side, cap, cut), out_shape=jax.S...]
    unnamed x7 -> x1, local copies, waits for them, and re-layouts: 4.03 us -> 1.88 us
where the time goes in v2:
time: 116 us; the launch traced here: 115 us
  Pallas kernels  114 us (98%)
  local copies, waits for them, and re-layouts  1.88 us (2%)
    pallas_call x1, Pallas kernels, shards(): pl.pallas_call(functools.partial(kernel, side, cap, cut), out_shape=jax.S...  114 us

profile of v2, /device:TPU:518, one launch (start us, length us, event | category | flops | bytes accessed | tf_op | source)
XLA Modules:
  0.0 115.5 jit_solution(673567378514490416)
XLA Ops:
  0.0 113.6 %shard_map.73 = bf16[128,2048]{1,0:T(8,128)(2,1)} custom-call(bf16[128,2048]{1,0:T(8,128)(2,1)} %tokens_ref.1, f32[1,2048]{1,0:T(1,128)} %bitcast.3, s32[2,128]{1,0:T(2,128)} %bitcast.4, f32[2,128]{1,0:T(2,128)} %bitcast.5, bf16[1,2048,256]{2,1,0:T(8,128)(2,1)} %wg_hbm.1, bf16[1,2048,256]{2,1,0:T(8,128)(2,1)} %wu_hbm.1, bf16[1,256,2048]{2,1,0:T(8,128)(2,1)} %wd_hbm.1), custom_call_target="tpu_custom_call" | custom-call | tf_op jit(solution)/shard_map/pallas_call | solution.py:329
  113.6 1.9 %copy.9 = bf16[128,2048]{1,0:T(8,128)(2,1)} copy(bf16[128,2048]{1,0:T(8,128)(2,1)} %shard_map.73) | data formatting | bytes 1048576

commit v3 on v2

v3 whole, which is shorter than its diff:
```python
import functools
import math

import jax
import jax.numpy as jnp
from jax import lax
from jax.experimental import pallas as pl
from jax.experimental.pallas import tpu as pltpu
from jax.sharding import PartitionSpec as P

N_GROUPS = 4
MESH = pl.DeviceIdType.MESH
BF16 = jnp.bfloat16
F32 = jnp.float32


def kernel(
    side,
    cap,
    cut,
    tokens_ref,
    gain_ref,
    ids_ref,
    gates_ref,
    wg_hbm,
    wu_hbm,
    wd_hbm,
    out_ref,
    info,
    infos,
    weigh,
    weigh_own,
    normed_a,
    normed_b,
    tok_a,
    tok_b,
    stage_a,
    stage_b,
    mid_a,
    mid_b,
    recv_a,
    recv_b,
    outs_a,
    outs_b,
    back_a,
    back_b,
    gath_a,
    gath_b,
    part_a,
    part_b,
    land_a,
    land_b,
    wg,
    wu,
    wd,
    local_sem,
    swap_sem,
    info_sem,
    tok_sem,
    relay_sem,
    turn_sem,
    line_sem,
    cross_sem,
    gath_sem,
    part_sem,
):
    n_ep = side * side
    half = side // 2
    pairs = half
    own, far = side - 2, side - 1
    ep = lax.axis_index("ep")
    tp = lax.axis_index("tp")
    my, mx = ep // side, lax.rem(ep, side)
    n_tok = tokens_ref.shape[0]
    line = side * cap
    rows = 2 * line
    groups = [(2 * c, 2) for c in range(pairs - 1)] + [(own, 1), (far, 1)]

    def shift(p):
        k = p // 2
        return jnp.where(k == half - 1, p % 2 * half, jnp.where(p % 2 == 0, k + 1, side - 1 - k))

    def place(d):
        near = jnp.where(d < half, 2 * (d - 1), 2 * (side - d) - 1)
        return jnp.where(d == 0, own, jnp.where(d == half, far, near))

    def at_column(d):
        return my * side + lax.rem(mx + d + side, side)

    def at_row(d):
        return lax.rem(my + d + side, side) * side + mx

    def in_row(p, sign):
        return at_column(sign * shift(p))

    def in_column(q, sign):
        return at_row(sign * shift(q))

    def others(do):
        @pl.loop(0, side - 1)
        def _(i):
            do(jnp.where(i == own, far, i))

    def remote(src, dst, sems, at, target):
        return pltpu.make_async_remote_copy(
            src_ref=src,
            dst_ref=dst,
            send_sem=sems.at[(0, *at)],
            recv_sem=sems.at[(1, *at)],
            device_id={"ep": target},
            device_id_type=MESH,
        )

    def step(axis, way, far_by):
        return (at_column, at_row)[axis](far_by * (1 - 2 * way))

    normed = (normed_a, normed_b)
    tok, stage, mid = (tok_a, tok_b), (stage_a, stage_b), (mid_a, mid_b)

    def tell(axis, way):
        return remote(info, infos.at[axis, way], info_sem, (axis, way), step(axis, way, 1))

    def give(axis, way):
        return remote(normed[axis], tok[axis].at[way], tok_sem, (axis, way), step(axis, way, 1))

    def relay(axis, way, b):
        at = (axis, way, b)
        if b < 2:
            src, dst = stage[axis].at[way, pl.ds(b * side, side)], mid[axis].at[2 + 2 * b + way]
        else:
            src = stage[axis].at[way, pl.ds(2 * side, half)]
            dst = mid[axis].at[far, pl.ds(way * half, half)]
        return remote(src, dst, relay_sem, at, step(axis, way, b + 1))

    def turn(axis, g, i):
        first, count = groups[g]
        some = pl.ds(first, count)
        if axis == 0:
            return remote(mid_a.at[some, i], recv_a.at[some, i], turn_sem, (0, g, i), in_column(i, 1))
        return remote(mid_b.at[some, i], recv_b.at[i, some], turn_sem, (1, g, i), in_row(i, 1))

    def in1_a(c, q):
        two = pl.ds(2 * c, 2)
        return remote(outs_a.at[two, q], back_a.at[two, q], cross_sem, (0, c, q), in_column(q, -1))

    def in1_b(p):
        return remote(outs_b.at[p], back_b.at[p], line_sem, (0, p), in_row(p, -1))

    back, gath, part, land = (back_a, back_b), (gath_a, gath_b), (part_a, part_b), (land_a, land_b)
    wide = (cut, tokens_ref.shape[1] - cut)

    def piece(axis, h):
        return pl.ds(h * (wide[axis] // 2), wide[axis] // 2)

    def gather(axis, way, b, n):
        at = (axis, way, b, n)
        target = step(axis, way, -(b + 1))
        i = far if b == 2 else 2 + 2 * b + way
        low = pl.ds(way * half, half) if b == 2 else pl.ds(0, side)
        into = pl.ds(b * side, half if b == 2 else side)
        if axis == 0:
            lanes = piece(0, n)
            return remote(back_a.at[i, low, :, lanes], gath_a.at[way, into, :, lanes], gath_sem, at, target)
        lanes = pl.ds(0, wide[1]) if n == 2 else piece(1, n)
        if b < 2:
            first = 0 if n == 2 else half
            low, into = pl.ds(first, half), pl.ds(b * side + first, half)
        return remote(back_b.at[low, i, :, lanes], gath_b.at[way, into, :, lanes], gath_sem, at, target)

    early_b = [(way, b, 2) for b in range(3) for way in range(2) if b < 2 or way == 0]

    def late_b(n):
        return [(way, b, n) for b in range(3) for way in range(2) if b < 2 or way == 1]

    def whole_a(n):
        return [(way, b, n) for b in range(3) for way in range(2)]

    def hand(axis, way, h):
        lanes = piece(axis, h)
        return remote(
            part[axis].at[way, :, lanes],
            land[axis].at[way, :, lanes],
            part_sem,
            (axis, way, h),
            step(axis, way, -1),
        )

    barrier = pltpu.get_barrier_semaphore()

    @pl.loop(1, side)
    def _(d):
        pl.semaphore_signal(barrier, inc=1, device_id={"ep": at_column(d)}, device_id_type=MESH)
        pl.semaphore_signal(barrier, inc=1, device_id={"ep": at_row(d)}, device_id_type=MESH)

    pl.semaphore_signal(barrier, inc=1, device_id={"tp": 1 - tp}, device_id_type=MESH)

    local = [
        pltpu.make_async_copy(src.at[0], dst.at[tp], local_sem.at[i])
        for i, (src, dst) in enumerate(((wg_hbm, wg), (wu_hbm, wu), (wd_hbm, wd)))
    ]
    for copy in local:
        copy.start()

    values = tokens_ref[...].astype(F32)
    scale = lax.rsqrt(jnp.mean(values * values, axis=-1, keepdims=True) + 1e-06)
    whole = (values * scale * gain_ref[...]).astype(BF16)
    normed_a[...] = whole[:, :cut]
    normed_b[...] = whole[:, cut:]

    pl.semaphore_wait(barrier, 2 * side - 1)
    for axis in range(2):
        for way in range(2):
            give(axis, way).start()

    ids = ids_ref[...]
    gates = gates_ref[...]
    below = lax.broadcasted_iota(jnp.int32, (n_ep, n_tok), 0)
    hots = [(ids[k : k + 1] == below).astype(F32) for k in range(ids.shape[0])]
    earlier = (
        lax.broadcasted_iota(jnp.int32, (n_tok, n_tok), 0)
        < lax.broadcasted_iota(jnp.int32, (n_tok, n_tok), 1)
    ).astype(BF16)
    before = jnp.dot(sum(hots).astype(BF16), earlier, preferred_element_type=F32)

    slots = []
    info[...] = jnp.zeros_like(info)
    for k, hot in enumerate(hots):
        e = ids[k : k + 1]
        nth = jnp.sum(before * hot, axis=0, keepdims=True).astype(jnp.int32)
        q = place((e // side - my + side) % side)
        p = place((e % side - mx + side) % side)
        slots.append((p * side + q) * cap + nth)
        info[k : k + 1] = slots[k].astype(F32)
        info[len(hots) + k : len(hots) + k + 1] = gates[k : k + 1]
    for axis in range(2):
        for way in range(2):
            tell(axis, way).start()

    def slot_of(axis, at, r):
        return at * line + r if axis == 0 else r // cap * line + at * cap + r % cap

    def choose(names, wanted, value):
        hit = sum((name == wanted).astype(F32) for name in names).astype(BF16)
        return jnp.dot(hit, value, preferred_element_type=F32).astype(BF16)

    def weigh_into(ref, names, wanted, shares):
        high = [g.astype(BF16).astype(F32) for g in shares]
        for n, split in enumerate((high, [g - h for g, h in zip(shares, high)])):
            ref[n] = sum(jnp.where(name == wanted, g, 0.0) for name, g in zip(names, split)).astype(BF16)

    def mix(ref, rows_of, value):
        return sum(
            lax.dot_general(ref[n, rows_of], value, (((0,), (0,)), ((), ())), preferred_element_type=F32)
            for n in range(2)
        )

    r = lax.broadcasted_iota(jnp.int32, (line, n_tok), 0)
    for axis in range(2):
        weigh_into(weigh_own.at[axis], slots, slot_of(axis, own, r), [gates[k : k + 1] for k in range(len(slots))])
        mine = choose(slots, slot_of(axis, own, r), normed[axis][...])
        mid[axis][own] = mine.reshape(side, cap, -1)

    def turn_group(g):
        def do(i):
            turn(0, g, i).start()
            turn(1, g, i).start()

        others(do)

    turn_group(pairs - 1)

    for copy in local:
        copy.wait()
    swaps = [
        pltpu.make_async_remote_copy(
            src_ref=ref.at[tp],
            dst_ref=ref.at[tp],
            send_sem=swap_sem.at[0, i],
            recv_sem=swap_sem.at[1, i],
            device_id={"tp": 1 - tp},
            device_id_type=MESH,
        )
        for i, ref in enumerate((wg, wu, wd))
    ]
    for swap in swaps:
        swap.start()

    r = lax.broadcasted_iota(jnp.int32, (3 * line + line // 2, n_tok), 0)
    for way in range(2):
        for axis in range(2):
            b = r // line
            inner = r % line + jnp.where(b == 3, way * (line // 2), 0)
            wanted = slot_of(axis, jnp.where(b == 3, far, 2 * b + way), inner)
            tell(axis, way).wait_recv()
            names = [infos[axis, way, k : k + 1].astype(jnp.int32) for k in range(len(slots))]
            give(axis, way).wait_recv()
            chosen = choose(names, wanted, tok[axis][way])
            mid[axis][way] = chosen[:line].reshape(side, cap, -1)
            stage[axis][way] = chosen[line:].reshape(2 * side + half, cap, -1)
            for b in range(3):
                relay(axis, way, b).start()
            shares = [infos[axis, way, len(slots) + k : len(slots) + k + 1] for k in range(len(slots))]
            weigh_into(weigh.at[axis, way], names, wanted, shares)

    turn_group(0)
    for b in range(3):
        for axis in range(2):
            for way in range(2):
                relay(axis, way, b).wait_recv()
        if b == 0:
            turn_group(1)

    def last_turns(i):
        for g in (2, pairs):
            turn(0, g, i).start()
            turn(1, g, i).start()

    others(last_turns)

    recv_a[:, own] = mid_a[:, own]
    recv_b[own] = mid_b[:, own]
    for swap in swaps:
        swap.wait()

    for c in range(pairs):
        for g in ((c,) if c < pairs - 1 else (c, c + 1)):
            others(lambda q: turn(0, g, q).wait_recv())
        for p in (2 * c, 2 * c + 1):
            if p != own:
                for g in range(len(groups)):
                    turn(1, g, p).wait_recv()

        two = pl.ds(2 * c, 2)
        taken_a = recv_a[two].reshape(rows, -1)
        taken_b = recv_b[two].reshape(rows, -1)
        total = None
        for j in range(wg.shape[0]):
            gate_act, up_act = (
                jnp.dot(taken_a, w[j, :cut], preferred_element_type=F32)
                + jnp.dot(taken_b, w[j, cut:], preferred_element_type=F32)
                for w in (wg, wu)
            )
            hidden = (gate_act / (1.0 + jnp.exp(-gate_act)) * up_act).astype(BF16)
            partial = jnp.dot(hidden, wd[j], preferred_element_type=F32).astype(BF16).astype(F32)
            total = partial if total is None else total + partial
        total = total.astype(BF16)
        outs_a[two] = total[:, :cut].reshape(2, side, cap, cut)
        outs_b[two] = total[:, cut:].reshape(2, side, cap, -1)
        others(lambda q: in1_a(c, q).start())
        for p in (2 * c, 2 * c + 1):
            if p != own:
                in1_b(p).start()

    back_a[:, own] = outs_a[:, own]
    back_b[own] = outs_b[own]

    def send(axis, which):
        for way, b, n in which:
            gather(axis, way, b, n).start()

    for c in range(pairs):
        for p in (2 * c, 2 * c + 1):
            if p != own:
                in1_b(p).wait_recv()
        others(lambda q: in1_a(c, q).wait_recv())
        if c == 1:
            send(1, early_b)
        if c:
            send(0, [(way, c - 1, 0) for way in range(2)])
    send(1, late_b(0))
    send(0, whole_a(1))
    send(1, late_b(1))

    def kept(axis, i, lanes):
        value = back_a[i, :, :, lanes] if axis == 0 else back_b[:, i, :, lanes]
        return value.reshape(line, -1)

    for h in range(2):
        for axis in range(2):
            lanes = piece(axis, h)
            for way in range(2):
                for w, b, n in (whole_a(h), late_b(h) + (early_b if h == 0 else []))[axis]:
                    if w == way:
                        gather(axis, way, b, n).wait_recv()
                got = mix(weigh.at[axis, way], pl.ds(0, line), kept(axis, way, lanes))
                got += mix(
                    weigh.at[axis, way],
                    pl.ds(line, 2 * line + line // 2),
                    gath[axis][way, :, :, lanes].reshape(2 * line + line // 2, -1),
                )
                part[axis][way, :, lanes] = got.astype(BF16)
                hand(axis, way, h).start()

    for h in range(2):
        for axis in range(2):
            lanes = piece(axis, h)
            got = mix(weigh_own.at[axis], pl.ds(0, line), kept(axis, own, lanes))
            for way in range(2):
                hand(axis, way, h).wait_recv()
                got += land[axis][way, :, lanes].astype(F32)
            out_ref[:, pl.ds(axis * cut + h * (wide[axis] // 2), wide[axis] // 2)] = got.astype(out_ref.dtype)

    for way, b, n in whole_a(0) + whole_a(1):
        gather(0, way, b, n).wait_send()
    for way, b, n in early_b + late_b(0) + late_b(1):
        gather(1, way, b, n).wait_send()
    for axis in range(2):
        for way in range(2):
            tell(axis, way).wait_send()
            give(axis, way).wait_send()
            for h in range(2):
                hand(axis, way, h).wait_send()
            for b in range(3):
                relay(axis, way, b).wait_send()

    def drain(i):
        in1_b(i).wait_send()
        for g in range(len(groups)):
            turn(0, g, i).wait_send()
            turn(1, g, i).wait_send()
        for c in range(pairs):
            in1_a(c, i).wait_send()

    others(drain)


def shards(n_ep, n_tp, tokens, norm_gain, expert_ids, gate_weights, w_gate, w_up, w_down):
    n_tok, width = tokens.shape
    top_count = expert_ids.shape[1]
    n_exp = w_gate.shape[0] * n_ep
    side = math.isqrt(n_ep)
    cap = top_count * (n_tok // 2) // (n_exp // N_GROUPS)
    cut = width // 2
    rows = 2 * side * cap
    hidden = w_gate.shape[2]
    vmem = pl.BlockSpec(memory_space=pltpu.VMEM)
    anywhere = pl.BlockSpec(memory_space=pl.ANY)
    dma = pltpu.SemaphoreType.DMA
    part_a = pltpu.VMEM((side, side, cap, cut), BF16)
    part_b = pltpu.VMEM((side, side, cap, width - cut), BF16)
    mixed = pl.pallas_call(
        functools.partial(kernel, side, cap, cut),
        out_shape=jax.ShapeDtypeStruct((n_tok, width), BF16),
        in_specs=[vmem] * 4 + [anywhere] * 3,
        out_specs=vmem,
        scratch_shapes=[
            pltpu.VMEM((8, n_tok), F32),
            pltpu.VMEM((2, 2, 8, n_tok), F32),
            pltpu.VMEM((2, 2, 2, 7 * side * cap // 2, n_tok), BF16),
            pltpu.VMEM((2, 2, side * cap, n_tok), BF16),
            pltpu.VMEM((n_tok, cut), BF16),
            pltpu.VMEM((n_tok, width - cut), BF16),
            pltpu.VMEM((2, n_tok, cut), BF16),
            pltpu.VMEM((2, n_tok, width - cut), BF16),
            pltpu.VMEM((2, 2 * side + side // 2, cap, cut), BF16),
            pltpu.VMEM((2, 2 * side + side // 2, cap, width - cut), BF16),
            *([part_a, part_b] * 4),
            pltpu.VMEM((2, 2 * side + side // 2, cap, cut), BF16),
            pltpu.VMEM((2, 2 * side + side // 2, cap, width - cut), BF16),
            *([pltpu.VMEM((2, n_tok, cut), BF16), pltpu.VMEM((2, n_tok, width - cut), BF16)] * 2),
            pltpu.VMEM((n_tp, width, hidden), BF16),
            pltpu.VMEM((n_tp, width, hidden), BF16),
            pltpu.VMEM((n_tp, hidden, width), BF16),
            dma((3,)),
            dma((2, 3)),
            dma((2, 2, 2)),
            dma((2, 2, 2)),
            dma((2, 2, 2, 3)),
            dma((2, 2, side // 2 + 1, side)),
            dma((2, 1, side)),
            dma((2, 1, side // 2, side)),
            dma((2, 2, 2, 3, 3)),
            dma((2, 2, 2, 2)),
        ],
        compiler_params=pltpu.CompilerParams(
            collective_id=0, has_side_effects=True, vmem_limit_bytes=60 * 1024 * 1024
        ),
    )(tokens, norm_gain.reshape(1, width), expert_ids.T, gate_weights.T, w_gate, w_up, w_down)
    return mixed


def solution(mesh):
    placed = (
        P(("grp", "ep", "tp"), None),
        P(),
        P(("grp", "ep", "tp"), None),
        P(("grp", "ep", "tp"), None),
        P("ep", None, "tp"),
        P("ep", None, "tp"),
        P("ep", "tp", None),
    )
    return jax.shard_map(
        functools.partial(shards, mesh.shape["ep"], mesh.shape["tp"]),
        mesh=mesh,
        in_specs=placed,
        out_specs=P(("grp", "ep", "tp"), None),
        check_vma=False,
    )
```

time: 116 us -> 113 us (0.974)
  Pallas kernels: 114 us -> 110 us
    pallas_call x1, Pallas kernels: 114 us -> 110 us  [shards(): pl.pallas_call(functools.partial(kernel, side, cap, cut), out_shape=jax.S...]
where the time goes in v3:
time: 113 us; the launch traced here: 112 us
  Pallas kernels  110 us (97%)
  local copies, waits for them, and re-layouts  1.88 us (2%)
    pallas_call x1, Pallas kernels, shards(): pl.pallas_call(functools.partial(kernel, side, cap, cut), out_shape=jax.S...  110 us

profile of v3, /device:TPU:518, one launch (start us, length us, event | category | flops | bytes accessed | tf_op | source)
XLA Modules:
  0.0 112.2 jit_solution(5401535960226101474)
XLA Ops:
  0.0 110.3 %shard_map.73 = bf16[128,2048]{1,0:T(8,128)(2,1)} custom-call(bf16[128,2048]{1,0:T(8,128)(2,1)} %tokens_ref.1, f32[1,2048]{1,0:T(1,128)} %bitcast.3, s32[2,128]{1,0:T(2,128)} %bitcast.4, f32[2,128]{1,0:T(2,128)} %bitcast.5, bf16[1,2048,256]{2,1,0:T(8,128)(2,1)} %wg_hbm.1, bf16[1,2048,256]{2,1,0:T(8,128)(2,1)} %wu_hbm.1, bf16[1,256,2048]{2,1,0:T(8,128)(2,1)} %wd_hbm.1), custom_call_target="tpu_custom_call" | custom-call | tf_op jit(solution)/shard_map/pallas_call | solution.py:441
  110.4 1.9 %copy.9 = bf16[128,2048]{1,0:T(8,128)(2,1)} copy(bf16[128,2048]{1,0:T(8,128)(2,1)} %shard_map.73) | data formatting | bytes 1048576

commit v4 on v3

--- a/solution.py
+++ b/solution.py
@@ -63,6 +63,7 @@
     cross_sem,
     gath_sem,
     part_sem,
+    word_sem,
 ):
     n_ep = side * side
     half = side // 2
@@ -187,10 +188,9 @@
 
     barrier = pltpu.get_barrier_semaphore()
 
-    @pl.loop(1, side)
-    def _(d):
-        pl.semaphore_signal(barrier, inc=1, device_id={"ep": at_column(d)}, device_id_type=MESH)
-        pl.semaphore_signal(barrier, inc=1, device_id={"ep": at_row(d)}, device_id_type=MESH)
+    for axis in range(2):
+        for way in range(2):
+            pl.semaphore_signal(barrier, inc=1, device_id={"ep": step(axis, way, 1)}, device_id_type=MESH)
 
     pl.semaphore_signal(barrier, inc=1, device_id={"tp": 1 - tp}, device_id_type=MESH)
 
@@ -207,13 +207,28 @@
     normed_a[...] = whole[:, :cut]
     normed_b[...] = whole[:, cut:]
 
-    pl.semaphore_wait(barrier, 2 * side - 1)
+    def pass_word(k):
+        for axis in range(2):
+            for way in range(2):
+                if k:
+                    pl.semaphore_wait(word_sem.at[k - 1, axis, way], 1)
+                if k < half - 1:
+                    pl.semaphore_signal(
+                        word_sem.at[k, axis, way],
+                        inc=1,
+                        device_id={"ep": step(axis, way, 1)},
+                        device_id_type=MESH,
+                    )
+
+    pl.semaphore_wait(barrier, 5)
+    pass_word(0)
     for axis in range(2):
         for way in range(2):
             give(axis, way).start()
 
     ids = ids_ref[...]
     gates = gates_ref[...]
+    pass_word(1)
     below = lax.broadcasted_iota(jnp.int32, (n_ep, n_tok), 0)
     hots = [(ids[k : k + 1] == below).astype(F32) for k in range(ids.shape[0])]
     earlier = (
@@ -235,6 +250,7 @@
     for axis in range(2):
         for way in range(2):
             tell(axis, way).start()
+    pass_word(2)
 
     def slot_of(axis, at, r):
         return at * line + r if axis == 0 else r // cap * line + at * cap + r % cap
@@ -267,6 +283,7 @@
 
         others(do)
 
+    pass_word(3)
     turn_group(pairs - 1)
 
     for copy in local:
@@ -354,6 +371,20 @@
     back_a[:, own] = outs_a[:, own]
     back_b[own] = outs_b[own]
 
+    for axis in range(2):
+        for way in range(2):
+            tell(axis, way).wait_send()
+            give(axis, way).wait_send()
+            for b in range(3):
+                relay(axis, way, b).wait_send()
+
+    def drain(i):
+        for g in range(len(groups)):
+            turn(0, g, i).wait_send()
+            turn(1, g, i).wait_send()
+
+    others(drain)
+
     def send(axis, which):
         for way, b, n in which:
             gather(axis, way, b, n).start()
@@ -370,6 +401,13 @@
     send(1, late_b(0))
     send(0, whole_a(1))
     send(1, late_b(1))
+
+    def drain_in1(i):
+        in1_b(i).wait_send()
+        for c in range(pairs):
+            in1_a(c, i).wait_send()
+
+    others(drain_in1)
 
     def kept(axis, i, lanes):
         value = back_a[i, :, :, lanes] if axis == 0 else back_b[:, i, :, lanes]
@@ -391,6 +429,11 @@
                 part[axis][way, :, lanes] = got.astype(BF16)
                 hand(axis, way, h).start()
 
+    for way, b, n in whole_a(0) + whole_a(1):
+        gather(0, way, b, n).wait_send()
+    for way, b, n in early_b + late_b(0) + late_b(1):
+        gather(1, way, b, n).wait_send()
+
     for h in range(2):
         for axis in range(2):
             lanes = piece(axis, h)
@@ -400,28 +443,10 @@
                 got += land[axis][way, :, lanes].astype(F32)
             out_ref[:, pl.ds(axis * cut + h * (wide[axis] // 2), wide[axis] // 2)] = got.astype(out_ref.dtype)
 
-    for way, b, n in whole_a(0) + whole_a(1):
-        gather(0, way, b, n).wait_send()
-    for way, b, n in early_b + late_b(0) + late_b(1):
-        gather(1, way, b, n).wait_send()
     for axis in range(2):
         for way in range(2):
-            tell(axis, way).wait_send()
-            give(axis, way).wait_send()
             for h in range(2):
                 hand(axis, way, h).wait_send()
-            for b in range(3):
-                relay(axis, way, b).wait_send()
-
-    def drain(i):
-        in1_b(i).wait_send()
-        for g in range(len(groups)):
-            turn(0, g, i).wait_send()
-            turn(1, g, i).wait_send()
-        for c in range(pairs):
-            in1_a(c, i).wait_send()
-
-    others(drain)
 
 
 def shards(n_ep, n_tp, tokens, norm_gain, expert_ids, gate_weights, w_gate, w_up, w_down):
@@ -471,6 +496,7 @@
             dma((2, 1, side // 2, side)),
             dma((2, 2, 2, 3, 3)),
             dma((2, 2, 2, 2)),
+            pltpu.SemaphoreType.REGULAR((side // 2 - 1, 2, 2)),
         ],
         compiler_params=pltpu.CompilerParams(
             collective_id=0, has_side_effects=True, vmem_limit_bytes=60 * 1024 * 1024

time: 113 us -> 112 us (level)
  no operation moved by 1% of the time
where the time goes in v4:
time: 112 us; the launch traced here: 111 us
  Pallas kernels  109 us (97%)
  local copies, waits for them, and re-layouts  1.88 us (2%)
    pallas_call x1, Pallas kernels, shards(): pl.pallas_call(functools.partial(kernel, side, cap, cut), out_shape=jax.S...  109 us

profile of v4, /device:TPU:518, one launch (start us, length us, event | category | flops | bytes accessed | tf_op | source)
XLA Modules:
  0.0 111.4 jit_solution(16800521519574190001)
XLA Ops:
  0.0 109.5 %shard_map.73 = bf16[128,2048]{1,0:T(8,128)(2,1)} custom-call(bf16[128,2048]{1,0:T(8,128)(2,1)} %tokens_ref.1, f32[1,2048]{1,0:T(1,128)} %bitcast.3, s32[2,128]{1,0:T(2,128)} %bitcast.4, f32[2,128]{1,0:T(2,128)} %bitcast.5, bf16[1,2048,256]{2,1,0:T(8,128)(2,1)} %wg_hbm.1, bf16[1,2048,256]{2,1,0:T(8,128)(2,1)} %wu_hbm.1, bf16[1,256,2048]{2,1,0:T(8,128)(2,1)} %wd_hbm.1), custom_call_target="tpu_custom_call" | custom-call | tf_op jit(solution)/shard_map/pallas_call | solution.py:466
  109.5 1.9 %copy.9 = bf16[128,2048]{1,0:T(8,128)(2,1)} copy(bf16[128,2048]{1,0:T(8,128)(2,1)} %shard_map.73) | data formatting | bytes 1048576
